TPU v7x, 256 devices: a whole 4x4x8 slice. The times are simulated.
256 devices in a mesh: ep: 16 (over y, x), tp: 16 (over z, core).
Axes of the slice: x: 4, y: 4, z: 8, core: 2. Of those that a mesh axis runs over, the one named last changes fastest.
Arguments:
- hidden_in: bfloat16 [256, 4096], P('ep'), may hold values from -6 to 6
- attn_gain: float32 [4096], replicated, may hold values from 0.1 to 1.9
- query_weight: bfloat16 [4096, 4096], P('ep', 'tp'), may hold values from -0.09375 to 0.09375
- key_weight: bfloat16 [4096, 2048], P('ep', 'tp'), may hold values from -0.09375 to 0.09375
- value_weight: bfloat16 [4096, 2048], P('ep', 'tp'), may hold values from -0.09375 to 0.09375
- query_gain: float32 [128], replicated, may hold values from 0.1 to 1.9
- key_gain: float32 [128], replicated, may hold values from 0.1 to 1.9
- head_offset: float32 [32], P('tp'), may hold values from -7 to -2
- key_cache: bfloat16 [256, 1024, 2048], P('ep', None, 'tp'), may hold values from -6 to 6
- value_cache: bfloat16 [256, 1024, 2048], P('ep', None, 'tp'), may hold values from -6 to 6
- lengths: int32 [256], P('ep'), may hold values from 1 to 1024
- out_weight: bfloat16 [4096, 4096], P('tp', 'ep'), may hold values from -0.375 to 0.375
- expert_gain: float32 [4096], replicated, may hold values from 0.1 to 1.9
- routes: int32 [256, 2], P('ep'), may hold values from 0 to 15, all different within a row; in each aligned block of 16 rows (0 to 15, 16 to 31, ...) at most 4 rows name the same one
- route_weights: float32 [256, 2], P('ep'), may hold values from 0.1 to 1
- gate_weight: bfloat16 [16, 4096, 2048], P('ep', None, 'tp'), may hold values from -0.09375 to 0.09375
- up_weight: bfloat16 [16, 4096, 2048], P('ep', None, 'tp'), may hold values from -0.09375 to 0.09375
- down_weight: bfloat16 [16, 2048, 4096], P('ep', 'tp'), may hold values from -0.125 to 0.125
Outputs:
- layer_out: bfloat16 [256, 4096], P('ep', 'tp')
- fresh_keys: bfloat16 [256, 2048], P('ep', 'tp')
- fresh_values: bfloat16 [256, 2048], P('ep', 'tp')
Inputs may be any that keep to these rules, and one draw needn't show every extreme that they name: `routes`: each row names 2 different experts. Among the rows of one index of ep (16 rows) no expert is named more than 4 times, a bound that some block reaches.
All inputs are finite; a program needn't handle non-finite values.
Results may differ from a plain program's by a relative error of at most 0.018.
Values may be sent and summed in bfloat16 or wider, within the bound.
A program may use at most 64 MiB of HBM per device.

v0:
```python
import jax
import jax.numpy as jnp
from jax import lax
from jax.sharding import PartitionSpec as P

EPSILON = 1e-06


def split_up(shard, dim, size):
    shape = shard.shape
    tiles = shard.reshape(*shape[:dim], size, shape[dim] // size, *shape[dim + 1 :])
    return jnp.moveaxis(tiles, dim, 0)


def sent_and_summed(shard, axis, dim):
    size = lax.axis_size(axis)
    tiles = lax.all_to_all(split_up(shard, dim, size), axis, 0, 0, tiled=True)
    return jnp.sum(tiles.astype(jnp.float32), axis=0)


def joined_along(tiles, dim):
    tiles = jnp.moveaxis(tiles, 0, dim)
    shape = tiles.shape
    return tiles.reshape(*shape[:dim], shape[dim] * shape[dim + 1], *shape[dim + 2 :])


def sent_to_all(shard, axis):
    size = lax.axis_size(axis)
    return lax.all_to_all(
        jnp.broadcast_to(shard[None], (size, *shard.shape)), axis, 0, 0, tiled=True
    )


def gather_directly(shard, axis, dim):
    return joined_along(sent_to_all(shard, axis), dim)


def over_copies(shard, axis):
    return sent_to_all(shard, axis).sum(axis=0)


def norm_rows(values, gain):
    meansq = jnp.mean(values * values, axis=-1, keepdims=True)
    return values * lax.rsqrt(meansq + EPSILON) * gain


def body(
    hidden_in,
    attn_gain,
    query_weight,
    key_weight,
    value_weight,
    query_gain,
    key_gain,
    head_offset,
    key_cache,
    value_cache,
    lengths,
    out_weight,
    expert_gain,
    routes,
    route_weights,
    gate_weight,
    up_weight,
    down_weight,
):
    count_ep = lax.axis_size("ep")
    count_tp = lax.axis_size("tp")
    seqs_here = hidden_in.shape[0]
    width = hidden_in.shape[1]
    head_dim = query_gain.shape[0]
    query_cols = query_weight.shape[1]
    pair_cols = key_weight.shape[1]
    kv_here = pair_cols // head_dim
    groups = query_cols // pair_cols
    cache_len = key_cache.shape[1]
    x_float = hidden_in.astype(jnp.float32)
    normed = norm_rows(x_float, attn_gain).astype(jnp.bfloat16)
    slices = lax.all_to_all(normed, "ep", split_axis=1, concat_axis=0, tiled=True)
    summed = sent_and_summed(
        jnp.concatenate(
            [
                jnp.dot(slices, query_weight, preferred_element_type=jnp.float32),
                jnp.dot(slices, key_weight, preferred_element_type=jnp.float32),
                jnp.dot(slices, value_weight, preferred_element_type=jnp.float32),
            ],
            axis=1,
        ).astype(jnp.bfloat16),
        "ep",
        0,
    )
    query_raw = summed[:, :query_cols].astype(jnp.bfloat16)
    key_raw = summed[:, query_cols : query_cols + pair_cols].astype(jnp.bfloat16)
    fresh_values = summed[:, query_cols + pair_cols :].astype(jnp.bfloat16)
    query = norm_rows(
        query_raw.astype(jnp.float32).reshape(seqs_here, query_cols // head_dim, head_dim),
        query_gain,
    ).astype(jnp.bfloat16)
    fresh_keys = norm_rows(
        key_raw.astype(jnp.float32).reshape(seqs_here, kv_here, head_dim), key_gain
    ).astype(jnp.bfloat16)
    grouped = query.reshape(seqs_here, kv_here, groups, head_dim)
    cached_keys = key_cache.reshape(seqs_here, cache_len, kv_here, head_dim)
    cached_values = value_cache.reshape(seqs_here, cache_len, kv_here, head_dim)
    scores = jnp.einsum("bkgd,bskd->bkgs", grouped, cached_keys, preferred_element_type=jnp.float32)
    scores = scores * head_dim ** (-0.5) + head_offset.reshape(kv_here, groups)[None, :, :, None]
    positions = lax.broadcasted_iota(jnp.int32, (1, 1, 1, cache_len), 3)
    live = positions < lengths[:, None, None, None]
    breaks = jnp.where(live, jax.nn.softplus(scores), 0.0)
    suffix = lax.cumsum(breaks, axis=3, reverse=True) - breaks
    stick = jnp.where(live, jnp.exp(jax.nn.log_sigmoid(scores) - suffix), 0.0).astype(jnp.bfloat16)
    attended = jnp.einsum(
        "bkgs,bskd->bkgd", stick, cached_values, preferred_element_type=jnp.float32
    )
    attended = attended.astype(jnp.bfloat16).reshape(seqs_here, query_cols)
    terms = jnp.dot(
        gather_directly(attended, "ep", 0), out_weight, preferred_element_type=jnp.float32
    )
    partial_value = lax.all_to_all(
        terms.astype(jnp.bfloat16), "ep", split_axis=0, concat_axis=1, tiled=True
    ).astype(terms.dtype)
    top = routes.shape[1]
    capacity = seqs_here * top * 2 // count_ep
    slots_all = count_ep * capacity
    flat = routes.reshape(-1)
    onehot = (flat[:, None] == lax.broadcasted_iota(jnp.int32, (1, count_ep), 1)).astype(jnp.int32)
    before = jnp.cumsum(onehot, axis=0) - onehot
    rank = jnp.sum(before * onehot, axis=1)
    slot = flat * capacity + rank
    match = (slot[:, None] == lax.broadcasted_iota(jnp.int32, (1, slots_all), 1)).astype(
        jnp.float32
    )
    match = match.reshape(seqs_here, top, slots_all)
    dispatch = jnp.sum(match, axis=1).astype(jnp.bfloat16)
    combine = jnp.sum(match * route_weights[:, :, None], axis=1)
    share_width = width // count_tp
    col_start = lax.axis_index("tp") * share_width
    projected_share = sent_and_summed(partial_value.astype(jnp.bfloat16), "tp", 1)
    own_share = lax.dynamic_slice_in_dim(x_float, col_start, share_width, 1)
    residual_share = (own_share + projected_share).astype(jnp.bfloat16)
    share_float = residual_share.astype(jnp.float32)
    squares = over_copies(jnp.sum(share_float * share_float, axis=1), "tp")
    gain_share = lax.dynamic_slice_in_dim(expert_gain, col_start, share_width, 0)
    expert_share = (
        share_float * lax.rsqrt(squares / width + EPSILON)[:, None] * gain_share
    ).astype(jnp.bfloat16)
    outgoing = jnp.einsum(
        "sj,sd->jd", dispatch, expert_share, preferred_element_type=jnp.float32
    ).astype(jnp.bfloat16)
    moved = lax.all_to_all(outgoing, "ep", split_axis=0, concat_axis=0, tiled=True)
    arrived = lax.all_gather(moved, "tp", axis=1, tiled=True)
    gate = jnp.dot(arrived, gate_weight[0], preferred_element_type=jnp.float32)
    upward = jnp.dot(arrived, up_weight[0], preferred_element_type=jnp.float32)
    hidden = (jax.nn.silu(gate) * upward).astype(jnp.bfloat16)
    expert_terms = jnp.dot(hidden, down_weight[0], preferred_element_type=jnp.float32)
    expert_out = sent_and_summed(expert_terms.astype(jnp.bfloat16), "tp", 1).astype(jnp.bfloat16)
    returned = lax.all_to_all(expert_out, "ep", split_axis=0, concat_axis=0, tiled=True)
    mixed = jnp.dot(combine, returned.astype(jnp.float32), precision=lax.Precision.HIGHEST)
    layer_out = (residual_share.astype(jnp.float32) + mixed).astype(jnp.bfloat16)
    return (layer_out, fresh_keys.reshape(seqs_here, pair_cols), fresh_values)


def solution(mesh):
    placed = (
        P("ep", None),
        P(),
        P("ep", "tp"),
        P("ep", "tp"),
        P("ep", "tp"),
        P(),
        P(),
        P("tp"),
        P("ep", None, "tp"),
        P("ep", None, "tp"),
        P("ep"),
        P("tp", "ep"),
        P(),
        P("ep", None),
        P("ep", None),
        P("ep", None, "tp"),
        P("ep", None, "tp"),
        P("ep", "tp", None),
    )
    return jax.shard_map(
        body,
        mesh=mesh,
        in_specs=placed,
        out_specs=(P("ep", "tp"), P("ep", "tp"), P("ep", "tp")),
        check_vma=False,
    )
```

profile of v0, /device:TPU:1, one launch (start us, length us, event | category | flops | bytes accessed | tf_op | source)
XLA Modules:
  0.0 199.3 jit_solution(7542754235354447465)
XLA Ops:
  0.6 0.0 copy-start
  0.6 1.1 multiply_reduce_fusion
  1.8 1.0 multiply_convert_fusion
  2.8 14.2 %all_to_all.79 = bf16[16,16,256]{2,0,1:T(8,128)(2,1)S(1)} all-to-all(bf16[16,16,256]{2,0,1:T(8,128)(2,1)S(1)} %bitcast.66), channel_id=1, replica_groups=mesh['ep'=16,'tp'=16] {'ep'}, dimensions={1} | all-to-all | bytes 262144 | tf_op jit(solution)/shard_map/all_to_all | solution.py:79
  17.1 1.0 convolution_convert_fusion.4
  18.1 1.0 convolution_convert_fusion.3
  19.1 1.1 convolution_convert_fusion.2
  20.2 0.7 pad_maximum_fusion
  20.9 3.5 %all-to-all-start.1 = ((bf16[16,16,512]{2,1,0:T(8,128)(2,1)}), bf16[16,16,512]{2,1,0:T(8,128)(2,1)S(1)}, u32[]{:S(2)}, u32[]{:S(2)}) async-start(bf16[16,16,512]{2,1,0:T(8,128)(2,1)} %pad_maximum_fusion), calls=%async_computation.1 | async-start | bytes 524288 | tf_op jit(solution)/shard_map/all_to_all | solution.py:17
  24.5 0.7 iota_compare_fusion
  25.2 6.8 %all-to-all-done.1 = bf16[16,16,512]{2,1,0:T(8,128)(2,1)S(1)} async-done(((bf16[16,16,512]{2,1,0:T(8,128)(2,1)}), bf16[16,16,512]{2,1,0:T(8,128)(2,1)S(1)}, u32[]{:S(2)}, u32[]{:S(2)}) %all-to-all-start.1) | async-done | bytes 262176 | tf_op jit(solution)/shard_map/all_to_all | solution.py:17
  32.1 0.1 multiply_reduce_fusion.1
  32.2 3.4 %fusion.11 = (f32[16,2,1024]{2,1,0:T(2,128)S(1)}, f32[16,2,1024]{2,1,0:T(2,128)S(1)}) fusion(pred[16,1024]{1,0:T(8,128)(4,1)S(1)} %iota_compare_fusion, f32[2]{0:T(128)} %param.25, bf16[16,1024,128]{2,1,0:T(8,128)(2,1)} %param.26, f32[16,2,128]{2,1,0:T(2,128)S(1)} %reshape.212, f32[128]{0:T(128)} %param.23, f32[16,2]{1,0:T(8,128)S(1)} %add_rsqrt_fusion), kind=kOutput, calls=%fused_computation.27 | convolution fusion | flops 8695808 | bytes 4489864 | tf_op jit(solution)/shard_map/bkgd,bskd->bkgs/dot_general | solution.py:105
  35.6 0.0 copy-start.4
  35.6 0.0 copy-start.3
  35.6 0.1 reshape.204
  35.8 0.0 copy-start.1
  35.8 39.6 %reduce-window.6 = f32[16,1,2,8,128]{4,3,2,1,0:T(8,128)S(1)} reduce-window(f32[16,1,2,8,128]{4,3,2,1,0:T(8,128)S(1)} %bitcast.67, f32[]{:T(128)} %constant.22.clone.1), window={size=1x1x1x1x128 pad=0_0x0_0x0_0x0_0x0_127}, to_apply=%region_3.0 | reduce-window | flops 4161536 | bytes 262148 | tf_op jit(solution)/shard_map/reduce-window
  75.4 0.1 reshape.205
  75.5 0.0 copy-start.5
  75.5 0.2 copy.64
  75.7 0.1 copy.65
  75.8 0.1 broadcast.120
  75.9 0.1 reshape.208
  76.0 0.0 copy-start.2
  76.0 3.4 %convolution_convert_fusion.6 = bf16[16,2,128]{2,1,0:T(2,128)(2,1)S(1)} fusion(bf16[16,1024,128]{2,1,0:T(8,128)(2,1)} %param.27, pred[16,1024]{1,0:T(8,128)(4,1)S(1)} %iota_compare_fusion, f32[16,2,1024]{2,1,0:T(2,128)S(1)} %reshape.205, f32[16,2,1024]{2,1,0:T(2,128)S(1)} %reshape.208, f32[16,2,1024]{2,1,0:T(2,128)S(1)} %get-tuple-element.8), kind=kOutput, calls=%fused_computation.12 | convolution fusion | flops 9048064 | bytes 4612096 | tf_op jit(solution)/shard_map/bkgs,bskd->bkgd/dot_general | solution.py:112
  79.3 0.7 broadcast_in_dim.22
  80.0 3.5 %all-to-all-start.2 = ((bf16[16,16,256]{2,1,0:T(8,128)(2,1)}), bf16[16,16,256]{2,1,0:T(8,128)(2,1)S(1)}, u32[]{:S(2)}, u32[]{:S(2)}) async-start(bf16[16,16,256]{2,1,0:T(8,128)(2,1)} %broadcast_in_dim.22), calls=%async_computation.2 | async-start | bytes 262144 | tf_op jit(solution)/shard_map/all_to_all | solution.py:29
  83.5 0.1 copy.66
  83.6 0.1 eq.29
  83.7 6.6 %all-to-all-done.2 = bf16[16,16,256]{2,1,0:T(8,128)(2,1)S(1)} async-done(((bf16[16,16,256]{2,1,0:T(8,128)(2,1)}), bf16[16,16,256]{2,1,0:T(8,128)(2,1)S(1)}, u32[]{:S(2)}, u32[]{:S(2)}) %all-to-all-start.2) | async-done | bytes 131104 | tf_op jit(solution)/shard_map/all_to_all | solution.py:29
  90.3 0.8 convolution_convert_fusion.1
  91.2 4.2 %all-to-all-start.3 = ((bf16[16,16,256]{2,1,0:T(8,128)(2,1)}), bf16[16,16,256]{2,1,0:T(8,128)(2,1)}, u32[]{:S(2)}, u32[]{:S(2)}) async-start(bf16[16,16,256]{2,1,0:T(8,128)(2,1)} %bitcast.8), calls=%async_computation.3 | async-start | bytes 262144 | tf_op jit(solution)/shard_map/all_to_all | solution.py:119
  95.3 0.1 fusion.28
  95.4 0.1 reduce_window_sum.25
  95.5 6.7 %all-to-all-done.3 = bf16[16,16,256]{2,1,0:T(8,128)(2,1)} async-done(((bf16[16,16,256]{2,1,0:T(8,128)(2,1)}), bf16[16,16,256]{2,1,0:T(8,128)(2,1)}, u32[]{:S(2)}, u32[]{:S(2)}) %all-to-all-start.3) | async-done | bytes 131104 | tf_op jit(solution)/shard_map/all_to_all | solution.py:119
  102.2 14.0 %all-to-all-start.4 = ((bf16[16,16,256]{2,1,0:T(8,128)(2,1)}), bf16[16,16,256]{2,1,0:T(8,128)(2,1)S(1)}, u32[]{:S(2)}, u32[]{:S(2)}) async-start(bf16[16,16,256]{2,1,0:T(8,128)(2,1)} %all-to-all-done.3), calls=%async_computation.4 | async-start | bytes 262144 | tf_op jit(solution)/shard_map/all_to_all | solution.py:17
  116.2 0.2 select_reduce_fusion.1
  116.4 0.0 copy-done.1
  116.4 0.1 reduce_sum.109
  116.5 0.1 copy.67
  116.6 8.5 %all-to-all-done.4 = bf16[16,16,256]{2,1,0:T(8,128)(2,1)S(1)} async-done(((bf16[16,16,256]{2,1,0:T(8,128)(2,1)}), bf16[16,16,256]{2,1,0:T(8,128)(2,1)S(1)}, u32[]{:S(2)}, u32[]{:S(2)}) %all-to-all-start.4) | async-done | bytes 131104 | tf_op jit(solution)/shard_map/all_to_all | solution.py:17
  125.1 0.1 fusion.24
  125.2 0.6 broadcast_in_dim.23
  125.8 3.4 %all-to-all-start.5 = ((f32[16,1,16]{2,1,0:T(1,128)}), f32[16,1,16]{2,1,0:T(1,128)S(1)}, u32[]{:S(2)}, u32[]{:S(2)}) async-start(f32[16,1,16]{2,1,0:T(1,128)} %broadcast_in_dim.23), calls=%async_computation.5 | async-start | bytes 16384 | tf_op jit(solution)/shard_map/all_to_all | solution.py:29
  129.2 0.1 convert_reduce_fusion.1
  129.3 0.8 dynamic_slice.7
  130.1 5.9 %all-to-all-done.5 = f32[16,1,16]{2,1,0:T(1,128)S(1)} async-done(((f32[16,1,16]{2,1,0:T(1,128)}), f32[16,1,16]{2,1,0:T(1,128)S(1)}, u32[]{:S(2)}, u32[]{:S(2)}) %all-to-all-start.5) | async-done | bytes 1056 | tf_op jit(solution)/shard_map/all_to_all | solution.py:29
  136.0 0.2 convolution_convert_fusion.5
  136.2 9.3 %all_to_all.80 = bf16[16,4,256]{2,1,0:T(4,128)(2,1)S(1)} all-to-all(bf16[16,4,256]{2,1,0:T(4,128)(2,1)S(1)} %all_to_all.63), channel_id=1, replica_groups=mesh['ep'=16,'tp'=16] {'ep'}, dimensions={0} | all-to-all | bytes 65536 | tf_op jit(solution)/shard_map/all_to_all | solution.py:150
  145.5 18.0 %all_gather.3 = bf16[64,4096]{1,0:T(8,128)(2,1)S(1)} all-gather(bf16[64,256]{1,0:T(8,128)(2,1)S(1)} %all_to_all.65), channel_id=1, replica_groups=mesh['ep'=16,'tp'=16] {'tp'}, dimensions={1}, use_global_device_ids=true | all-gather | bytes 557056 | tf_op jit(solution)/shard_map/all_gather | solution.py:151
  163.5 1.5 fusion.6
  165.1 0.6 convolution_convert_fusion
  165.7 0.8 copy.76
  166.6 4.2 %all-to-all-start.7 = ((bf16[16,64,256]{2,1,0:T(8,128)(2,1)}), bf16[16,64,256]{2,1,0:T(8,128)(2,1)S(1)}, u32[]{:S(2)}, u32[]{:S(2)}) async-start(bf16[16,64,256]{2,1,0:T(8,128)(2,1)} %bitcast.58), calls=%async_computation.7 | async-start | bytes 1048576 | tf_op jit(solution)/shard_map/all_to_all | solution.py:17
  170.7 0.1 fusion.29
  170.9 17.1 %all-to-all-done.7 = bf16[16,64,256]{2,1,0:T(8,128)(2,1)S(1)} async-done(((bf16[16,64,256]{2,1,0:T(8,128)(2,1)}), bf16[16,64,256]{2,1,0:T(8,128)(2,1)S(1)}, u32[]{:S(2)}, u32[]{:S(2)}) %all-to-all-start.7) | async-done | bytes 524320 | tf_op jit(solution)/shard_map/all_to_all | solution.py:17
  187.9 0.1 reduce_sum.114
  188.0 0.6 all_to_all.67
  188.6 3.5 %all-to-all-start.8 = ((bf16[16,4,256]{2,1,0:T(4,128)(2,1)}), bf16[16,4,256]{2,1,0:T(4,128)(2,1)S(1)}, u32[]{:S(2)}, u32[]{:S(2)}) async-start(bf16[16,4,256]{2,1,0:T(4,128)(2,1)} %all_to_all.67), calls=%async_computation.8 | async-start | bytes 65536 | tf_op jit(solution)/shard_map/all_to_all | solution.py:157
  192.2 0.7 fusion.31
  192.8 0.6 slice.27
  193.4 5.1 %all-to-all-done.8 = bf16[16,4,256]{2,1,0:T(4,128)(2,1)S(1)} async-done(((bf16[16,4,256]{2,1,0:T(4,128)(2,1)}), bf16[16,4,256]{2,1,0:T(4,128)(2,1)S(1)}, u32[]{:S(2)}, u32[]{:S(2)}) %all-to-all-start.8) | async-done | bytes 32800 | tf_op jit(solution)/shard_map/all_to_all | solution.py:157
  198.6 0.7 fusion.2
  (25 shorter events, 0.3 us)
Async XLA Ops:
  0.6 164.5 %copy-start = (bf16[1,128,4096]{2,1,0:T(8,128)(2,1)S(1)}, bf16[1,128,4096]{2,1,0:T(8,128)(2,1)}, u32[]{:S(2)}) copy-start(bf16[1,128,4096]{2,1,0:T(8,128)(2,1)} %param.35) | copy-start | bytes 3145732
  20.9 11.0 %all-to-all-start.1 = ((bf16[16,16,512]{2,1,0:T(8,128)(2,1)}), bf16[16,16,512]{2,1,0:T(8,128)(2,1)S(1)}, u32[]{:S(2)}, u32[]{:S(2)}) async-start(bf16[16,16,512]{2,1,0:T(8,128)(2,1)} %pad_maximum_fusion), calls=%async_computation.1 | async-start | bytes 524288 | tf_op jit(solution)/shard_map/all_to_all | solution.py:17
  35.6 47.9 %copy-start.4 = (s32[16,2]{0,1:T(2,128)S(1)}, s32[16,2]{0,1:T(2,128)}, u32[]{:S(2)}) copy-start(s32[16,2]{0,1:T(2,128)} %param.31) | copy-start | bytes 388
  35.6 54.7 %copy-start.3 = (bf16[256,256]{1,0:T(8,128)(2,1)S(1)}, bf16[256,256]{1,0:T(8,128)(2,1)}, u32[]{:S(2)}) copy-start(bf16[256,256]{1,0:T(8,128)(2,1)} %param.29) | copy-start | bytes 393220
  35.8 80.6 %copy-start.1 = (bf16[16,4096]{1,0:T(8,128)(2,1)S(1)}, bf16[16,4096]{1,0:T(8,128)(2,1)}, u32[]{:S(2)}) copy-start(bf16[16,4096]{1,0:T(8,128)(2,1)} %param.18) | copy-start | bytes 393220
  75.5 53.7 %copy-start.5 = (f32[16,2]{0,1:T(2,128)S(1)}, f32[16,2]{0,1:T(2,128)}, u32[]{:S(2)}) copy-start(f32[16,2]{0,1:T(2,128)} %param.32) | copy-start | bytes 388
  76.0 89.1 %copy-start.2 = (bf16[1,4096,128]{2,1,0:T(8,128)(2,1)S(1)}, bf16[1,4096,128]{2,1,0:T(8,128)(2,1)}, u32[]{:S(2)}) copy-start(bf16[1,4096,128]{2,1,0:T(8,128)(2,1)} %param.34) | copy-start | bytes 3145732
  80.0 10.3 %all-to-all-start.2 = ((bf16[16,16,256]{2,1,0:T(8,128)(2,1)}), bf16[16,16,256]{2,1,0:T(8,128)(2,1)S(1)}, u32[]{:S(2)}, u32[]{:S(2)}) async-start(bf16[16,16,256]{2,1,0:T(8,128)(2,1)} %broadcast_in_dim.22), calls=%async_computation.2 | async-start | bytes 262144 | tf_op jit(solution)/shard_map/all_to_all | solution.py:29
  91.2 11.0 %all-to-all-start.3 = ((bf16[16,16,256]{2,1,0:T(8,128)(2,1)}), bf16[16,16,256]{2,1,0:T(8,128)(2,1)}, u32[]{:S(2)}, u32[]{:S(2)}) async-start(bf16[16,16,256]{2,1,0:T(8,128)(2,1)} %bitcast.8), calls=%async_computation.3 | async-start | bytes 262144 | tf_op jit(solution)/shard_map/all_to_all | solution.py:119
  102.2 22.9 %all-to-all-start.4 = ((bf16[16,16,256]{2,1,0:T(8,128)(2,1)}), bf16[16,16,256]{2,1,0:T(8,128)(2,1)S(1)}, u32[]{:S(2)}, u32[]{:S(2)}) async-start(bf16[16,16,256]{2,1,0:T(8,128)(2,1)} %all-to-all-done.3), calls=%async_computation.4 | async-start | bytes 262144 | tf_op jit(solution)/shard_map/all_to_all | solution.py:17
  125.8 10.1 %all-to-all-start.5 = ((f32[16,1,16]{2,1,0:T(1,128)}), f32[16,1,16]{2,1,0:T(1,128)S(1)}, u32[]{:S(2)}, u32[]{:S(2)}) async-start(f32[16,1,16]{2,1,0:T(1,128)} %broadcast_in_dim.23), calls=%async_computation.5 | async-start | bytes 16384 | tf_op jit(solution)/shard_map/all_to_all | solution.py:29
  136.0 56.2 %copy-start.6 = (f32[128]{0:T(128)S(1)}, f32[128]{0:T(128)}, u32[]{:S(2)}) copy-start(f32[128]{0:T(128)} %param.24) | copy-start | bytes 1540
  166.6 21.4 %all-to-all-start.7 = ((bf16[16,64,256]{2,1,0:T(8,128)(2,1)}), bf16[16,64,256]{2,1,0:T(8,128)(2,1)S(1)}, u32[]{:S(2)}, u32[]{:S(2)}) async-start(bf16[16,64,256]{2,1,0:T(8,128)(2,1)} %bitcast.58), calls=%async_computation.7 | async-start | bytes 1048576 | tf_op jit(solution)/shard_map/all_to_all | solution.py:17
  188.6 9.9 %all-to-all-start.8 = ((bf16[16,4,256]{2,1,0:T(4,128)(2,1)}), bf16[16,4,256]{2,1,0:T(4,128)(2,1)S(1)}, u32[]{:S(2)}, u32[]{:S(2)}) async-start(bf16[16,4,256]{2,1,0:T(4,128)(2,1)} %all_to_all.67), calls=%async_computation.8 | async-start | bytes 65536 | tf_op jit(solution)/shard_map/all_to_all | solution.py:157
where the time goes:
time: 200 us; the launch traced here: 199 us
  waiting for transfers between devices  56.7 us (28%)
  other arithmetic  44.9 us (22%)
  blocking collectives  41.5 us (21%)
  starting transfers between devices  36.3 us (18%)
  matrix products  13.8 us (7%)
  local copies, waits for them, and re-layouts  5.17 us (3%)
    another operation x2, other arithmetic  39.7 us
    all_to_all x3, waiting for transfers between devices, sent_and_summed(): tiles = lax.all_to_all(split_up(shard, dim, size), axis, 0, 0, tiled=True)  32.3 us
    all_to_all x3, starting transfers between devices, sent_and_summed(): tiles = lax.all_to_all(split_up(shard, dim, size), axis, 0, 0, tiled=True)  21.7 us
    all_gather x1, blocking collectives, body(): arrived = lax.all_gather(moved, 'tp', axis=1, tiled=True)  18 us
    all_to_all x1, blocking collectives, body(): lax.all_to_all(normed, 'ep', split_axis=1, concat_axis=0, tiled=True)  14.2 us
    all_to_all x2, waiting for transfers between devices, sent_to_all(): lax.all_to_all(jnp.broadcast_to(shard[None], (size, *shard.shape)), axis,...  12.5 us
    all_to_all x1, blocking collectives, body(): lax.all_to_all(outgoing, 'ep', split_axis=0, concat_axis=0, tiled=True)  9.26 us
    all_to_all x2, starting transfers between devices, sent_to_all(): lax.all_to_all(jnp.broadcast_to(shard[None], (size, *shard.shape)), axis,...  6.88 us
  transfers between devices with their start and end apart: 7, of which 7 were waited for; matrix products, arithmetic and copies ran while one was open for 2% of the time, Pallas kernels for 0%

commit v1 on v0

--- a/solution.py
+++ b/solution.py
@@ -4,6 +4,19 @@
 from jax.sharding import PartitionSpec as P
 
 EPSILON = 1e-06
+
+
+def gather_around(array, axis, dim):
+    ways = lax.axis_size(axis)
+    up = [(d, (d + 1) % ways) for d in range(ways)]
+    down = [(d, (d - 1) % ways) for d in range(ways)]
+    earlier, later = ([array], [array])
+    for _ in range(ways // 2):
+        earlier.append(lax.ppermute(earlier[-1], axis, up))
+    for _ in range((ways - 1) // 2):
+        later.append(lax.ppermute(later[-1], axis, down))
+    line = jnp.concatenate([*earlier[::-1], *later[1:]], axis=dim)
+    return jnp.roll(line, (lax.axis_index(axis) - ways // 2) * array.shape[dim], axis=dim)
 
 
 def split_up(shard, dim, size):
@@ -148,7 +161,7 @@
         "sj,sd->jd", dispatch, expert_share, preferred_element_type=jnp.float32
     ).astype(jnp.bfloat16)
     moved = lax.all_to_all(outgoing, "ep", split_axis=0, concat_axis=0, tiled=True)
-    arrived = lax.all_gather(moved, "tp", axis=1, tiled=True)
+    arrived = gather_around(moved, "tp", 1)
     gate = jnp.dot(arrived, gate_weight[0], preferred_element_type=jnp.float32)
     upward = jnp.dot(arrived, up_weight[0], preferred_element_type=jnp.float32)
     hidden = (jax.nn.silu(gate) * upward).astype(jnp.bfloat16)

time: 200 us -> 225 us (1.12)
  starting transfers between devices: 36.3 us -> 66.9 us
  blocking collectives: 41.5 us -> 23.5 us
  waiting for transfers between devices: 56.7 us -> 63 us
  local copies, waits for them, and re-layouts: 5.17 us -> 10.3 us
    ppermute x0 -> x15, starting transfers between devices: none -> 27.7 us  [the longest x7 21.1 us: gather_around(): later.append(lax.ppermute(later[-1], axis, down))]
    all_gather x1 -> x0, blocking collectives: 18 us -> none  [body(): arrived = lax.all_gather(moved, 'tp', axis=1, tiled=True)]
    ppermute x0 -> x15, waiting for transfers between devices: none -> 6.65 us  [the longest x8 5.39 us: gather_around(): earlier.append(lax.ppermute(earlier[-1], axis, up))]
    unnamed x16 -> x57, local copies, waits for them, and re-layouts: 0.14 us -> 5.27 us
    all_to_all x3, starting transfers between devices: 21.7 us -> 24.7 us  [sent_and_summed(): tiles = lax.all_to_all(split_up(shard, dim, size), axis, 0, 0, tiled=True)]
  transfers between devices with their start and end apart: 7 -> 22, of which waited for: 7 -> 19; matrix products, arithmetic and copies ran while one was open for 2% -> 3% of each run, Pallas kernels for 0% -> 0%
where the time goes in v1:
time: 225 us; the launch traced here: 224 us
  starting transfers between devices  66.9 us (30%)
  waiting for transfers between devices  63 us (28%)
  other arithmetic  45.5 us (20%)
  blocking collectives  23.5 us (10%)
  matrix products  13.8 us (6%)
  local copies, waits for them, and re-layouts  10.3 us (5%)
    another operation x2, other arithmetic  39.7 us
    all_to_all x3, waiting for transfers between devices, sent_and_summed(): tiles = lax.all_to_all(split_up(shard, dim, size), axis, 0, 0, tiled=True)  32.4 us
    all_to_all x3, starting transfers between devices, sent_and_summed(): tiles = lax.all_to_all(split_up(shard, dim, size), axis, 0, 0, tiled=True)  24.7 us
    ppermute x7, starting transfers between devices, gather_around(): later.append(lax.ppermute(later[-1], axis, down))  21.1 us
    all_to_all x1, blocking collectives, body(): lax.all_to_all(normed, 'ep', split_axis=1, concat_axis=0, tiled=True)  14.2 us
    all_to_all x2, waiting for transfers between devices, sent_to_all(): lax.all_to_all(jnp.broadcast_to(shard[None], (size, *shard.shape)), axis,...  12.1 us
    all_to_all x1, blocking collectives, body(): lax.all_to_all(outgoing, 'ep', split_axis=0, concat_axis=0, tiled=True)  9.26 us
    all_to_all x2, starting transfers between devices, sent_to_all(): lax.all_to_all(jnp.broadcast_to(shard[None], (size, *shard.shape)), axis,...  6.84 us
  transfers between devices with their start and end apart: 22, of which 19 were waited for; matrix products, arithmetic and copies ran while one was open for 3% of the time, Pallas kernels for 0%

profile of v1, /device:TPU:1, one launch (start us, length us, event | category | flops | bytes accessed | tf_op | source)
XLA Modules:
  0.0 224.1 jit_solution(4876654007091405034)
XLA Ops:
  0.6 1.1 multiply_reduce_fusion
  1.8 1.0 multiply_convert_fusion
  2.8 14.2 %all_to_all.79 = bf16[16,16,256]{2,0,1:T(8,128)(2,1)S(1)} all-to-all(bf16[16,16,256]{2,0,1:T(8,128)(2,1)S(1)} %bitcast.67), channel_id=1, replica_groups=mesh['ep'=16,'tp'=16] {'ep'}, dimensions={1} | all-to-all | bytes 262144 | tf_op jit(solution)/shard_map/all_to_all | solution.py:92
  17.1 1.0 convolution_convert_fusion.4
  18.1 1.0 convolution_convert_fusion.3
  19.1 1.1 convolution_convert_fusion.2
  20.2 0.7 pad_maximum_fusion
  20.9 3.5 %all-to-all-start.1 = ((bf16[16,16,512]{2,1,0:T(8,128)(2,1)}), bf16[16,16,512]{2,1,0:T(8,128)(2,1)S(1)}, u32[]{:S(2)}, u32[]{:S(2)}) async-start(bf16[16,16,512]{2,1,0:T(8,128)(2,1)} %pad_maximum_fusion), calls=%async_computation.1 | async-start | bytes 524288 | tf_op jit(solution)/shard_map/all_to_all | solution.py:30
  24.5 0.7 iota_compare_fusion
  25.2 6.8 %all-to-all-done.1 = bf16[16,16,512]{2,1,0:T(8,128)(2,1)S(1)} async-done(((bf16[16,16,512]{2,1,0:T(8,128)(2,1)}), bf16[16,16,512]{2,1,0:T(8,128)(2,1)S(1)}, u32[]{:S(2)}, u32[]{:S(2)}) %all-to-all-start.1) | async-done | bytes 262176 | tf_op jit(solution)/shard_map/all_to_all | solution.py:30
  32.2 3.4 %fusion.12 = (f32[16,2,1024]{2,1,0:T(2,128)S(1)}, f32[16,2,1024]{2,1,0:T(2,128)S(1)}) fusion(pred[16,1024]{1,0:T(8,128)(4,1)S(1)} %iota_compare_fusion, f32[2]{0:T(128)} %param.25, bf16[16,1024,128]{2,1,0:T(8,128)(2,1)} %param.26, f32[16,2,128]{2,1,0:T(2,128)S(1)} %reshape.212, f32[128]{0:T(128)} %param.23, f32[16,2]{1,0:T(8,128)S(1)} %add_rsqrt_fusion), kind=kOutput, calls=%fused_computation.28 | convolution fusion | flops 8695808 | bytes 4489864 | tf_op jit(solution)/shard_map/bkgd,bskd->bkgs/dot_general | solution.py:118
  35.8 39.6 %reduce-window.6 = f32[16,1,2,8,128]{4,3,2,1,0:T(8,128)S(1)} reduce-window(f32[16,1,2,8,128]{4,3,2,1,0:T(8,128)S(1)} %bitcast.68, f32[]{:T(128)} %constant.59.clone.1), window={size=1x1x1x1x128 pad=0_0x0_0x0_0x0_0x0_127}, to_apply=%region_3.0 | reduce-window | flops 4161536 | bytes 262148 | tf_op jit(solution)/shard_map/reduce-window
  76.0 3.3 %convolution_convert_fusion.6 = bf16[16,2,128]{2,1,0:T(2,128)(2,1)S(1)} fusion(bf16[16,1024,128]{2,1,0:T(8,128)(2,1)} %param.27, pred[16,1024]{1,0:T(8,128)(4,1)S(1)} %iota_compare_fusion, f32[16,2,1024]{2,1,0:T(2,128)S(1)} %reshape.205, f32[16,2,1024]{2,1,0:T(2,128)S(1)} %reshape.208, f32[16,2,1024]{2,1,0:T(2,128)S(1)} %get-tuple-element.8), kind=kOutput, calls=%fused_computation.10 | convolution fusion | flops 9048064 | bytes 4612096 | tf_op jit(solution)/shard_map/bkgs,bskd->bkgd/dot_general | solution.py:125
  79.3 0.7 broadcast_in_dim.22
  79.9 3.5 %all-to-all-start.2 = ((bf16[16,16,256]{2,1,0:T(8,128)(2,1)}), bf16[16,16,256]{2,1,0:T(8,128)(2,1)S(1)}, u32[]{:S(2)}, u32[]{:S(2)}) async-start(bf16[16,16,256]{2,1,0:T(8,128)(2,1)} %broadcast_in_dim.22), calls=%async_computation.2 | async-start | bytes 262144 | tf_op jit(solution)/shard_map/all_to_all | solution.py:42
  83.6 6.6 %all-to-all-done.2 = bf16[16,16,256]{2,1,0:T(8,128)(2,1)S(1)} async-done(((bf16[16,16,256]{2,1,0:T(8,128)(2,1)}), bf16[16,16,256]{2,1,0:T(8,128)(2,1)S(1)}, u32[]{:S(2)}, u32[]{:S(2)}) %all-to-all-start.2) | async-done | bytes 131104 | tf_op jit(solution)/shard_map/all_to_all | solution.py:42
  90.3 0.8 convolution_convert_fusion.1
  91.1 4.2 %all-to-all-start.3 = ((bf16[16,16,256]{2,1,0:T(8,128)(2,1)}), bf16[16,16,256]{2,1,0:T(8,128)(2,1)}, u32[]{:S(2)}, u32[]{:S(2)}) async-start(bf16[16,16,256]{2,1,0:T(8,128)(2,1)} %bitcast.8), calls=%async_computation.3 | async-start | bytes 262144 | tf_op jit(solution)/shard_map/all_to_all | solution.py:132
  95.4 6.7 %all-to-all-done.3 = bf16[16,16,256]{2,1,0:T(8,128)(2,1)} async-done(((bf16[16,16,256]{2,1,0:T(8,128)(2,1)}), bf16[16,16,256]{2,1,0:T(8,128)(2,1)}, u32[]{:S(2)}, u32[]{:S(2)}) %all-to-all-start.3) | async-done | bytes 131104 | tf_op jit(solution)/shard_map/all_to_all | solution.py:132
  102.1 14.0 %all-to-all-start.4 = ((bf16[16,16,256]{2,1,0:T(8,128)(2,1)}), bf16[16,16,256]{2,1,0:T(8,128)(2,1)S(1)}, u32[]{:S(2)}, u32[]{:S(2)}) async-start(bf16[16,16,256]{2,1,0:T(8,128)(2,1)} %all-to-all-done.3), calls=%async_computation.4 | async-start | bytes 262144 | tf_op jit(solution)/shard_map/all_to_all | solution.py:30
  116.5 8.5 %all-to-all-done.4 = bf16[16,16,256]{2,1,0:T(8,128)(2,1)S(1)} async-done(((bf16[16,16,256]{2,1,0:T(8,128)(2,1)}), bf16[16,16,256]{2,1,0:T(8,128)(2,1)S(1)}, u32[]{:S(2)}, u32[]{:S(2)}) %all-to-all-start.4) | async-done | bytes 131104 | tf_op jit(solution)/shard_map/all_to_all | solution.py:30
  125.2 0.6 broadcast_in_dim.23
  125.8 3.3 %all-to-all-start.5 = ((f32[16,1,16]{2,1,0:T(1,128)}), f32[16,1,16]{2,1,0:T(1,128)S(1)}, u32[]{:S(2)}, u32[]{:S(2)}) async-start(f32[16,1,16]{2,1,0:T(1,128)} %broadcast_in_dim.23), calls=%async_computation.5 | async-start | bytes 16384 | tf_op jit(solution)/shard_map/all_to_all | solution.py:42
  129.1 0.7 convert_reduce_fusion.1
  129.8 0.8 dynamic_slice.11
  130.6 5.4 %all-to-all-done.5 = f32[16,1,16]{2,1,0:T(1,128)S(1)} async-done(((f32[16,1,16]{2,1,0:T(1,128)}), f32[16,1,16]{2,1,0:T(1,128)S(1)}, u32[]{:S(2)}, u32[]{:S(2)}) %all-to-all-start.5) | async-done | bytes 1056 | tf_op jit(solution)/shard_map/all_to_all | solution.py:42
  136.3 9.3 %all_to_all.80 = bf16[16,4,256]{2,1,0:T(4,128)(2,1)S(1)} all-to-all(bf16[16,4,256]{2,1,0:T(4,128)(2,1)S(1)} %all_to_all.63), channel_id=1, replica_groups=mesh['ep'=16,'tp'=16] {'ep'}, dimensions={0} | all-to-all | bytes 65536 | tf_op jit(solution)/shard_map/all_to_all | solution.py:163
  145.5 2.3 %collective-permute-start = (bf16[64,256]{1,0:T(8,128)(2,1)S(1)}, bf16[64,256]{1,0:T(8,128)(2,1)S(1)}, u32[]{:S(2)}, u32[]{:S(2)}) collective-permute-start(bf16[64,256]{1,0:T(8,128)(2,1)S(1)} %all_to_all.65), channel_id=1, source_target_pairs={{0,1},{1,2},{2,3},{3,4},{4,5},{5,6},{6,7},{7,8},{8,9},{9,10},{10,1... | collective-permute-start | bytes 98312 | tf_op jit(solution)/shard_map/ppermute | solution.py:15
  147.8 1.0 collective-permute-done
  148.8 2.3 %collective-permute-start.1 = (bf16[64,256]{1,0:T(8,128)(2,1)S(1)}, bf16[64,256]{1,0:T(8,128)(2,1)S(1)}, u32[]{:S(2)}, u32[]{:S(2)}) collective-permute-start(bf16[64,256]{1,0:T(8,128)(2,1)S(1)} %collective-permute-done), channel_id=1, source_target_pairs={{0,1},{1,2},{2,3},{3,4},{4,5},{5,6},{6,7},{7,8},{8,9},{9,10},{10,1... | collective-permute-start | bytes 98312 | tf_op jit(solution)/shard_map/ppermute | solution.py:15
  151.1 1.1 collective-permute-start.8
  152.2 0.7 collective-permute-done.1
  152.9 1.6 collective-permute-start.2
  154.5 2.3 %collective-permute-start.9 = (bf16[64,256]{1,0:T(8,128)(2,1)S(1)}, bf16[64,256]{1,0:T(8,128)(2,1)S(1)}, u32[]{:S(2)}, u32[]{:S(2)}) collective-permute-start(bf16[64,256]{1,0:T(8,128)(2,1)S(1)} %collective-permute-done.8), channel_id=1, source_target_pairs={{0,15},{1,0},{2,1},{3,2},{4,3},{5,4},{6,5},{7,6},{8,7},{9,8},{10,9... | collective-permute-start | bytes 98312 | tf_op jit(solution)/shard_map/ppermute | solution.py:17
  156.7 0.7 collective-permute-done.2
  157.4 0.4 collective-permute-start.3
  157.8 3.5 %collective-permute-start.10 = (bf16[64,256]{1,0:T(8,128)(2,1)S(1)}, bf16[64,256]{1,0:T(8,128)(2,1)S(1)}, u32[]{:S(2)}, u32[]{:S(2)}) collective-permute-start(bf16[64,256]{1,0:T(8,128)(2,1)S(1)} %collective-permute-done.9), channel_id=1, source_target_pairs={{0,15},{1,0},{2,1},{3,2},{4,3},{5,4},{6,5},{7,6},{8,7},{9,8},{10,9... | collective-permute-start | bytes 98312 | tf_op jit(solution)/shard_map/ppermute | solution.py:17
  161.3 0.7 collective-permute-done.3
  162.2 3.7 %collective-permute-start.11 = (bf16[64,256]{1,0:T(8,128)(2,1)S(1)}, bf16[64,256]{1,0:T(8,128)(2,1)S(1)}, u32[]{:S(2)}, u32[]{:S(2)}) collective-permute-start(bf16[64,256]{1,0:T(8,128)(2,1)S(1)} %collective-permute-done.10), channel_id=1, source_target_pairs={{0,15},{1,0},{2,1},{3,2},{4,3},{5,4},{6,5},{7,6},{8,7},{9,8},{10,9... | collective-permute-start | bytes 98312 | tf_op jit(solution)/shard_map/ppermute | solution.py:17
  165.8 0.7 collective-permute-done.4
  166.7 3.7 %collective-permute-start.12 = (bf16[64,256]{1,0:T(8,128)(2,1)S(1)}, bf16[64,256]{1,0:T(8,128)(2,1)S(1)}, u32[]{:S(2)}, u32[]{:S(2)}) collective-permute-start(bf16[64,256]{1,0:T(8,128)(2,1)S(1)} %collective-permute-done.11), channel_id=1, source_target_pairs={{0,15},{1,0},{2,1},{3,2},{4,3},{5,4},{6,5},{7,6},{8,7},{9,8},{10,9... | collective-permute-start | bytes 98312 | tf_op jit(solution)/shard_map/ppermute | solution.py:17
  170.4 0.7 collective-permute-done.5
  171.3 0.4 copy-done.4
  171.7 3.8 %collective-permute-start.13 = (bf16[64,256]{1,0:T(8,128)(2,1)S(1)}, bf16[64,256]{1,0:T(8,128)(2,1)S(1)}, u32[]{:S(2)}, u32[]{:S(2)}) collective-permute-start(bf16[64,256]{1,0:T(8,128)(2,1)S(1)} %collective-permute-done.12), channel_id=1, source_target_pairs={{0,15},{1,0},{2,1},{3,2},{4,3},{5,4},{6,5},{7,6},{8,7},{9,8},{10,9... | collective-permute-start | bytes 98312 | tf_op jit(solution)/shard_map/ppermute | solution.py:17
  175.6 0.8 collective-permute-done.13
  176.4 3.1 %collective-permute-start.14 = (bf16[64,256]{1,0:T(8,128)(2,1)S(1)}, bf16[64,256]{1,0:T(8,128)(2,1)S(1)}, u32[]{:S(2)}, u32[]{:S(2)}) collective-permute-start(bf16[64,256]{1,0:T(8,128)(2,1)S(1)} %collective-permute-done.13), channel_id=1, source_target_pairs={{0,15},{1,0},{2,1},{3,2},{4,3},{5,4},{6,5},{7,6},{8,7},{9,8},{10,9... | collective-permute-start | bytes 98312 | tf_op jit(solution)/shard_map/ppermute | solution.py:17
  179.5 0.8 collective-permute-done.7
  180.3 0.8 constant_dynamic-update-slice_fusion.31
  181.1 0.8 constant_dynamic-update-slice_fusion.30
  181.8 0.8 constant_dynamic-update-slice_fusion.29
  182.8 0.8 constant_dynamic-update-slice_fusion.15
  183.5 0.8 constant_dynamic-update-slice_fusion.14
  184.3 0.8 constant_dynamic-update-slice_fusion.13
  185.2 0.3 fusion.3
  185.6 1.8 convolution_convert_fusion
  187.4 0.8 copy.76
  188.3 7.2 %all-to-all-start.7 = ((bf16[16,64,256]{2,1,0:T(8,128)(2,1)}), bf16[16,64,256]{2,1,0:T(8,128)(2,1)S(1)}, u32[]{:S(2)}, u32[]{:S(2)}) async-start(bf16[16,64,256]{2,1,0:T(8,128)(2,1)} %bitcast.59), calls=%async_computation.7 | async-start | bytes 1048576 | tf_op jit(solution)/shard_map/all_to_all | solution.py:30
  195.5 17.2 %all-to-all-done.7 = bf16[16,64,256]{2,1,0:T(8,128)(2,1)S(1)} async-done(((bf16[16,64,256]{2,1,0:T(8,128)(2,1)}), bf16[16,64,256]{2,1,0:T(8,128)(2,1)S(1)}, u32[]{:S(2)}, u32[]{:S(2)}) %all-to-all-start.7) | async-done | bytes 524320 | tf_op jit(solution)/shard_map/all_to_all | solution.py:30
  212.8 0.6 all_to_all.67
  213.4 3.5 %all-to-all-start.8 = ((bf16[16,4,256]{2,1,0:T(4,128)(2,1)}), bf16[16,4,256]{2,1,0:T(4,128)(2,1)S(1)}, u32[]{:S(2)}, u32[]{:S(2)}) async-start(bf16[16,4,256]{2,1,0:T(4,128)(2,1)} %all_to_all.67), calls=%async_computation.8 | async-start | bytes 65536 | tf_op jit(solution)/shard_map/all_to_all | solution.py:170
  216.9 0.7 fusion.35
  217.6 0.6 slice.27
  218.2 5.1 %all-to-all-done.8 = bf16[16,4,256]{2,1,0:T(4,128)(2,1)S(1)} async-done(((bf16[16,4,256]{2,1,0:T(4,128)(2,1)}), bf16[16,4,256]{2,1,0:T(4,128)(2,1)S(1)}, u32[]{:S(2)}, u32[]{:S(2)}) %all-to-all-start.8) | async-done | bytes 32800 | tf_op jit(solution)/shard_map/all_to_all | solution.py:170
  223.4 0.7 fusion.1
  (96 shorter events, 2.9 us)
Async XLA Ops:
  0.6 184.9 %copy-start = (bf16[1,128,4096]{2,1,0:T(8,128)(2,1)S(1)}, bf16[1,128,4096]{2,1,0:T(8,128)(2,1)}, u32[]{:S(2)}) copy-start(bf16[1,128,4096]{2,1,0:T(8,128)(2,1)} %param.35) | copy-start | bytes 3145732
  20.9 11.0 %all-to-all-start.1 = ((bf16[16,16,512]{2,1,0:T(8,128)(2,1)}), bf16[16,16,512]{2,1,0:T(8,128)(2,1)S(1)}, u32[]{:S(2)}, u32[]{:S(2)}) async-start(bf16[16,16,512]{2,1,0:T(8,128)(2,1)} %pad_maximum_fusion), calls=%async_computation.1 | async-start | bytes 524288 | tf_op jit(solution)/shard_map/all_to_all | solution.py:30
  35.6 47.9 %copy-start.9 = (s32[16,2]{0,1:T(2,128)S(1)}, s32[16,2]{0,1:T(2,128)}, u32[]{:S(2)}) copy-start(s32[16,2]{0,1:T(2,128)} %param.31) | copy-start | bytes 388
  35.6 54.7 %copy-start.3 = (bf16[256,256]{1,0:T(8,128)(2,1)S(1)}, bf16[256,256]{1,0:T(8,128)(2,1)}, u32[]{:S(2)}) copy-start(bf16[256,256]{1,0:T(8,128)(2,1)} %param.29) | copy-start | bytes 393220
  35.7 80.6 %copy-start.1 = (bf16[16,4096]{1,0:T(8,128)(2,1)S(1)}, bf16[16,4096]{1,0:T(8,128)(2,1)}, u32[]{:S(2)}) copy-start(bf16[16,4096]{1,0:T(8,128)(2,1)} %param.18) | copy-start | bytes 393220
  75.4 53.7 %copy-start.10 = (f32[16,2]{0,1:T(2,128)S(1)}, f32[16,2]{0,1:T(2,128)}, u32[]{:S(2)}) copy-start(f32[16,2]{0,1:T(2,128)} %param.32) | copy-start | bytes 388
  75.9 109.3 %copy-start.2 = (bf16[1,4096,128]{2,1,0:T(8,128)(2,1)S(1)}, bf16[1,4096,128]{2,1,0:T(8,128)(2,1)}, u32[]{:S(2)}) copy-start(bf16[1,4096,128]{2,1,0:T(8,128)(2,1)} %param.34) | copy-start | bytes 3145732
  79.9 10.3 %all-to-all-start.2 = ((bf16[16,16,256]{2,1,0:T(8,128)(2,1)}), bf16[16,16,256]{2,1,0:T(8,128)(2,1)S(1)}, u32[]{:S(2)}, u32[]{:S(2)}) async-start(bf16[16,16,256]{2,1,0:T(8,128)(2,1)} %broadcast_in_dim.22), calls=%async_computation.2 | async-start | bytes 262144 | tf_op jit(solution)/shard_map/all_to_all | solution.py:42
  91.1 11.0 %all-to-all-start.3 = ((bf16[16,16,256]{2,1,0:T(8,128)(2,1)}), bf16[16,16,256]{2,1,0:T(8,128)(2,1)}, u32[]{:S(2)}, u32[]{:S(2)}) async-start(bf16[16,16,256]{2,1,0:T(8,128)(2,1)} %bitcast.8), calls=%async_computation.3 | async-start | bytes 262144 | tf_op jit(solution)/shard_map/all_to_all | solution.py:132
  102.1 22.9 %all-to-all-start.4 = ((bf16[16,16,256]{2,1,0:T(8,128)(2,1)}), bf16[16,16,256]{2,1,0:T(8,128)(2,1)S(1)}, u32[]{:S(2)}, u32[]{:S(2)}) async-start(bf16[16,16,256]{2,1,0:T(8,128)(2,1)} %all-to-all-done.3), calls=%async_computation.4 | async-start | bytes 262144 | tf_op jit(solution)/shard_map/all_to_all | solution.py:30
  125.2 10.9 %copy-start.7 = (bf16[16,256]{1,0:T(8,128)(2,1)}, bf16[16,256]{1,0:T(8,128)(2,1)S(1)}, u32[]{:S(2)}) copy-start(bf16[16,256]{1,0:T(8,128)(2,1)S(1)} %get-tuple-element.6) | copy-start | bytes 24580
  125.8 10.2 %all-to-all-start.5 = ((f32[16,1,16]{2,1,0:T(1,128)}), f32[16,1,16]{2,1,0:T(1,128)S(1)}, u32[]{:S(2)}, u32[]{:S(2)}) async-start(f32[16,1,16]{2,1,0:T(1,128)} %broadcast_in_dim.23), calls=%async_computation.5 | async-start | bytes 16384 | tf_op jit(solution)/shard_map/all_to_all | solution.py:42
  145.5 3.3 %collective-permute-start = (bf16[64,256]{1,0:T(8,128)(2,1)S(1)}, bf16[64,256]{1,0:T(8,128)(2,1)S(1)}, u32[]{:S(2)}, u32[]{:S(2)}) collective-permute-start(bf16[64,256]{1,0:T(8,128)(2,1)S(1)} %all_to_all.65), channel_id=1, source_target_pairs={{0,1},{1,2},{2,3},{3,4},{4,5},{5,6},{6,7},{7,8},{8,9},{9,10},{10,1... | collective-permute-start | bytes 98312 | tf_op jit(solution)/shard_map/ppermute | solution.py:15
  148.8 4.1 %collective-permute-start.1 = (bf16[64,256]{1,0:T(8,128)(2,1)S(1)}, bf16[64,256]{1,0:T(8,128)(2,1)S(1)}, u32[]{:S(2)}, u32[]{:S(2)}) collective-permute-start(bf16[64,256]{1,0:T(8,128)(2,1)S(1)} %collective-permute-done), channel_id=1, source_target_pairs={{0,1},{1,2},{2,3},{3,4},{4,5},{5,6},{6,7},{7,8},{8,9},{9,10},{10,1... | collective-permute-start | bytes 98312 | tf_op jit(solution)/shard_map/ppermute | solution.py:15
  151.1 3.3 %collective-permute-start.8 = (bf16[64,256]{1,0:T(8,128)(2,1)S(1)}, bf16[64,256]{1,0:T(8,128)(2,1)S(1)}, u32[]{:S(2)}, u32[]{:S(2)}) collective-permute-start(bf16[64,256]{1,0:T(8,128)(2,1)S(1)} %all_to_all.65), channel_id=1, source_target_pairs={{0,15},{1,0},{2,1},{3,2},{4,3},{5,4},{6,5},{7,6},{8,7},{9,8},{10,9... | collective-permute-start | bytes 98312 | tf_op jit(solution)/shard_map/ppermute | solution.py:17
  152.9 4.6 %collective-permute-start.2 = (bf16[64,256]{1,0:T(8,128)(2,1)S(1)}, bf16[64,256]{1,0:T(8,128)(2,1)S(1)}, u32[]{:S(2)}, u32[]{:S(2)}) collective-permute-start(bf16[64,256]{1,0:T(8,128)(2,1)S(1)} %collective-permute-done.1), channel_id=1, source_target_pairs={{0,1},{1,2},{2,3},{3,4},{4,5},{5,6},{6,7},{7,8},{8,9},{9,10},{10,1... | collective-permute-start | bytes 98312 | tf_op jit(solution)/shard_map/ppermute | solution.py:15
  154.5 3.3 %collective-permute-start.9 = (bf16[64,256]{1,0:T(8,128)(2,1)S(1)}, bf16[64,256]{1,0:T(8,128)(2,1)S(1)}, u32[]{:S(2)}, u32[]{:S(2)}) collective-permute-start(bf16[64,256]{1,0:T(8,128)(2,1)S(1)} %collective-permute-done.8), channel_id=1, source_target_pairs={{0,15},{1,0},{2,1},{3,2},{4,3},{5,4},{6,5},{7,6},{8,7},{9,8},{10,9... | collective-permute-start | bytes 98312 | tf_op jit(solution)/shard_map/ppermute | solution.py:17
  157.4 4.6 %collective-permute-start.3 = (bf16[64,256]{1,0:T(8,128)(2,1)S(1)}, bf16[64,256]{1,0:T(8,128)(2,1)S(1)}, u32[]{:S(2)}, u32[]{:S(2)}) collective-permute-start(bf16[64,256]{1,0:T(8,128)(2,1)S(1)} %collective-permute-done.2), channel_id=1, source_target_pairs={{0,1},{1,2},{2,3},{3,4},{4,5},{5,6},{6,7},{7,8},{8,9},{9,10},{10,1... | collective-permute-start | bytes 98312 | tf_op jit(solution)/shard_map/ppermute | solution.py:15
  157.8 4.3 %collective-permute-start.10 = (bf16[64,256]{1,0:T(8,128)(2,1)S(1)}, bf16[64,256]{1,0:T(8,128)(2,1)S(1)}, u32[]{:S(2)}, u32[]{:S(2)}) collective-permute-start(bf16[64,256]{1,0:T(8,128)(2,1)S(1)} %collective-permute-done.9), channel_id=1, source_target_pairs={{0,15},{1,0},{2,1},{3,2},{4,3},{5,4},{6,5},{7,6},{8,7},{9,8},{10,9... | collective-permute-start | bytes 98312 | tf_op jit(solution)/shard_map/ppermute | solution.py:17
  162.0 4.6 %collective-permute-start.4 = (bf16[64,256]{1,0:T(8,128)(2,1)S(1)}, bf16[64,256]{1,0:T(8,128)(2,1)S(1)}, u32[]{:S(2)}, u32[]{:S(2)}) collective-permute-start(bf16[64,256]{1,0:T(8,128)(2,1)S(1)} %collective-permute-done.3), channel_id=1, source_target_pairs={{0,1},{1,2},{2,3},{3,4},{4,5},{5,6},{6,7},{7,8},{8,9},{9,10},{10,1... | collective-permute-start | bytes 98312 | tf_op jit(solution)/shard_map/ppermute | solution.py:15
  162.2 4.6 %collective-permute-start.11 = (bf16[64,256]{1,0:T(8,128)(2,1)S(1)}, bf16[64,256]{1,0:T(8,128)(2,1)S(1)}, u32[]{:S(2)}, u32[]{:S(2)}) collective-permute-start(bf16[64,256]{1,0:T(8,128)(2,1)S(1)} %collective-permute-done.10), channel_id=1, source_target_pairs={{0,15},{1,0},{2,1},{3,2},{4,3},{5,4},{6,5},{7,6},{8,7},{9,8},{10,9... | collective-permute-start | bytes 98312 | tf_op jit(solution)/shard_map/ppermute | solution.py:17
  166.5 4.6 %collective-permute-start.5 = (bf16[64,256]{1,0:T(8,128)(2,1)S(1)}, bf16[64,256]{1,0:T(8,128)(2,1)S(1)}, u32[]{:S(2)}, u32[]{:S(2)}) collective-permute-start(bf16[64,256]{1,0:T(8,128)(2,1)S(1)} %collective-permute-done.4), channel_id=1, source_target_pairs={{0,1},{1,2},{2,3},{3,4},{4,5},{5,6},{6,7},{7,8},{8,9},{9,10},{10,1... | collective-permute-start | bytes 98312 | tf_op jit(solution)/shard_map/ppermute | solution.py:15
  166.7 4.6 %collective-permute-start.12 = (bf16[64,256]{1,0:T(8,128)(2,1)S(1)}, bf16[64,256]{1,0:T(8,128)(2,1)S(1)}, u32[]{:S(2)}, u32[]{:S(2)}) collective-permute-start(bf16[64,256]{1,0:T(8,128)(2,1)S(1)} %collective-permute-done.11), channel_id=1, source_target_pairs={{0,15},{1,0},{2,1},{3,2},{4,3},{5,4},{6,5},{7,6},{8,7},{9,8},{10,9... | collective-permute-start | bytes 98312 | tf_op jit(solution)/shard_map/ppermute | solution.py:17
  171.1 0.6 copy-start.4
  171.1 4.6 %collective-permute-start.6 = (bf16[64,256]{1,0:T(8,128)(2,1)S(1)}, bf16[64,256]{1,0:T(8,128)(2,1)S(1)}, u32[]{:S(2)}, u32[]{:S(2)}) collective-permute-start(bf16[64,256]{1,0:T(8,128)(2,1)S(1)} %collective-permute-done.5), channel_id=1, source_target_pairs={{0,1},{1,2},{2,3},{3,4},{4,5},{5,6},{6,7},{7,8},{8,9},{9,10},{10,1... | collective-permute-start | bytes 98312 | tf_op jit(solution)/shard_map/ppermute | solution.py:15
  171.7 4.7 %collective-permute-start.13 = (bf16[64,256]{1,0:T(8,128)(2,1)S(1)}, bf16[64,256]{1,0:T(8,128)(2,1)S(1)}, u32[]{:S(2)}, u32[]{:S(2)}) collective-permute-start(bf16[64,256]{1,0:T(8,128)(2,1)S(1)} %collective-permute-done.12), channel_id=1, source_target_pairs={{0,15},{1,0},{2,1},{3,2},{4,3},{5,4},{6,5},{7,6},{8,7},{9,8},{10,9... | collective-permute-start | bytes 98312 | tf_op jit(solution)/shard_map/ppermute | solution.py:17
  175.6 3.9 %copy-start.5 = (bf16[64,256]{1,0:T(8,128)(2,1)}, bf16[64,256]{1,0:T(8,128)(2,1)S(1)}, u32[]{:S(2)}) copy-start(bf16[64,256]{1,0:T(8,128)(2,1)S(1)} %collective-permute-done.6) | copy-start | bytes 98308
  175.6 4.7 %collective-permute-start.7 = (bf16[64,256]{1,0:T(8,128)(2,1)S(1)}, bf16[64,256]{1,0:T(8,128)(2,1)}, u32[]{:S(2)}, u32[]{:S(2)}) collective-permute-start(bf16[64,256]{1,0:T(8,128)(2,1)S(1)} %collective-permute-done.6), channel_id=1, source_target_pairs={{0,1},{1,2},{2,3},{3,4},{4,5},{5,6},{6,7},{7,8},{8,9},{9,10},{10,1... | collective-permute-start | bytes 98312 | tf_op jit(solution)/shard_map/ppermute | solution.py:15
  176.4 6.3 %collective-permute-start.14 = (bf16[64,256]{1,0:T(8,128)(2,1)S(1)}, bf16[64,256]{1,0:T(8,128)(2,1)S(1)}, u32[]{:S(2)}, u32[]{:S(2)}) collective-permute-start(bf16[64,256]{1,0:T(8,128)(2,1)S(1)} %collective-permute-done.13), channel_id=1, source_target_pairs={{0,15},{1,0},{2,1},{3,2},{4,3},{5,4},{6,5},{7,6},{8,7},{9,8},{10,9... | collective-permute-start | bytes 98312 | tf_op jit(solution)/shard_map/ppermute | solution.py:17
  185.1 31.9 %copy-start.11 = (f32[128]{0:T(128)S(1)}, f32[128]{0:T(128)}, u32[]{:S(2)}) copy-start(f32[128]{0:T(128)} %param.24) | copy-start | bytes 1540
  185.1 38.3 %copy-start.6 = (f32[16,64]{1,0:T(8,128)S(1)}, f32[16,64]{1,0:T(8,128)}, u32[]{:S(2)}) copy-start(f32[16,64]{1,0:T(8,128)} %get-tuple-element.4) | copy-start | bytes 12292
  185.1 38.3 %copy-start.8 = (bf16[16,256]{1,0:T(8,128)(2,1)S(1)}, bf16[16,256]{1,0:T(8,128)(2,1)}, u32[]{:S(2)}) copy-start(bf16[16,256]{1,0:T(8,128)(2,1)} %copy-done.7) | copy-start | bytes 24580
  188.3 24.5 %all-to-all-start.7 = ((bf16[16,64,256]{2,1,0:T(8,128)(2,1)}), bf16[16,64,256]{2,1,0:T(8,128)(2,1)S(1)}, u32[]{:S(2)}, u32[]{:S(2)}) async-start(bf16[16,64,256]{2,1,0:T(8,128)(2,1)} %bitcast.59), calls=%async_computation.7 | async-start | bytes 1048576 | tf_op jit(solution)/shard_map/all_to_all | solution.py:30
  213.4 9.9 %all-to-all-start.8 = ((bf16[16,4,256]{2,1,0:T(4,128)(2,1)}), bf16[16,4,256]{2,1,0:T(4,128)(2,1)S(1)}, u32[]{:S(2)}, u32[]{:S(2)}) async-start(bf16[16,4,256]{2,1,0:T(4,128)(2,1)} %all_to_all.67), calls=%async_computation.8 | async-start | bytes 65536 | tf_op jit(solution)/shard_map/all_to_all | solution.py:170
